TPU v7x, 32 devices: a whole 2x2x4 slice. The times are simulated.
32 devices in a mesh: sp: 8 (over z, y), tp: 4 (over x, core).
Axes of the slice: x: 2, y: 2, z: 4, core: 2. Of those that a mesh axis runs over, the one named last changes fastest.
Arguments:
- queries: bfloat16 [6144, 1536], P('sp', 'tp'), may hold values from -130 to 130, as said below
- keys: bfloat16 [6144, 512], P('sp', 'tp'), may hold values from -6 to 6
- values: bfloat16 [6144, 512], P('sp', 'tp'), may hold values from -6 to 6
- residual: bfloat16 [6144, 2048], P(('sp', 'tp')), may hold values from -6 to 6
- sinks: float32 [12], P('tp'), may hold values from 2 to 6
- out_weight: bfloat16 [1536, 2048], P('tp'), may hold values from -0.15625 to 0.15625
- up_weight: bfloat16 [2048, 8192], P('sp', 'tp'), may hold values from -0.125 to 0.125
- down_weight: bfloat16 [8192, 2048], P('tp', 'sp'), may hold values from -0.0625 to 0.0625
- gains: float32 [2, 2048], replicated, may hold values from 0.1 to 1.9
- biases: float32 [2, 2048], replicated, may hold values from -3 to 3
Outputs:
- layer_out: bfloat16 [6144, 2048], P(('sp', 'tp'))
Inputs may be any that keep to these rules, and one draw needn't show every extreme that they name: `queries`: entries of order one, with some rows far larger in some draws.
All inputs are finite; a program needn't handle non-finite values.
Results may differ from a plain program's by a relative error of at most 0.0095.
Values may be sent and summed in bfloat16 or wider, within the bound.
A program may use at most 128 MiB of HBM per device.

v0:
```python
import jax
import jax.numpy as jnp
from jax import lax
from jax.sharding import PartitionSpec as P

HEADS = 12
HEAD = 128
WINDOW = 128
deep_alpha = 1.6817928
norm_eps = 1e-05
neg_big = -1e30


def from_behind(block, axis, distance):
    devices = range(lax.axis_size(axis))
    route = [(i - distance, i) for i in devices if i - distance in devices]
    return lax.ppermute(block, axis, route)


def layer_norm(stream, gain, bias):
    mean = jnp.mean(stream, axis=-1, keepdims=True)
    spread = jnp.mean(jnp.square(stream - mean), axis=-1, keepdims=True)
    return ((stream - mean) * lax.rsqrt(spread + norm_eps) * gain + bias).astype(jnp.bfloat16)


def attend(queries, keys, values, before, sinks, offset, rank_tp):
    tokens = keys.shape[0]
    kv_local = keys.shape[1] // HEAD
    heads_local = sinks.shape[0]
    group = heads_local // kv_local
    blocks = tokens // WINDOW
    q_blocks = queries.reshape(blocks, WINDOW, kv_local, group, HEAD)
    key_ext = jnp.concatenate([before[0], keys], axis=0).reshape(tokens + WINDOW, kv_local, HEAD)
    val_ext = jnp.concatenate([before[1], values], axis=0).reshape(tokens + WINDOW, kv_local, HEAD)
    key_win = jnp.concatenate(
        [
            key_ext[:tokens].reshape(blocks, WINDOW, kv_local, HEAD),
            key_ext[WINDOW:].reshape(blocks, WINDOW, kv_local, HEAD),
        ],
        axis=1,
    )
    val_win = jnp.concatenate(
        [
            val_ext[:tokens].reshape(blocks, WINDOW, kv_local, HEAD),
            val_ext[WINDOW:].reshape(blocks, WINDOW, kv_local, HEAD),
        ],
        axis=1,
    )
    logits = jnp.einsum(
        "nqkgd,nskd->nkgqs", q_blocks, key_win, preferred_element_type=jnp.float32
    ) * HEAD ** (-0.5)
    q_index = jnp.arange(WINDOW, dtype=jnp.int32)[:, None]
    k_index = jnp.arange(2 * WINDOW, dtype=jnp.int32)[None, :]
    dist = q_index + WINDOW - k_index
    block_id = jnp.arange(blocks, dtype=jnp.int32)[:, None, None]
    key_pos = offset + block_id * WINDOW - WINDOW + k_index
    valid = (dist >= 0) & (dist < WINDOW) & (key_pos >= 0)
    heads = (jnp.arange(heads_local, dtype=jnp.int32) + rank_tp * heads_local).astype(jnp.float32)
    slopes = jnp.exp2(-8.0 * (heads + 1.0) / HEADS).reshape(kv_local, group)[:, :, None, None]
    logits = logits - slopes * dist.astype(jnp.float32)
    logits = jnp.where(valid[:, None, None], logits, neg_big)
    sink = sinks.reshape(kv_local, group)[:, :, None, None]
    top = jnp.maximum(jnp.max(logits, axis=-1, keepdims=True), sink)
    probs = jnp.exp(logits - top)
    denom = jnp.sum(probs, axis=-1, keepdims=True) + jnp.exp(sink - top)
    weight = (probs / denom).astype(jnp.bfloat16)
    attended = jnp.einsum("nkgqs,nskd->nqkgd", weight, val_win, preferred_element_type=jnp.float32)
    return attended.astype(jnp.bfloat16).reshape(tokens, heads_local * HEAD)


def on_device(
    queries, keys, values, residual, sinks, out_weight, up_weight, down_weight, gains, biases
):
    tokens = queries.shape[0]
    rank_tp = lax.axis_index("tp")
    up_full, down_full = (
        lax.all_gather(up_weight, "sp", axis=0, tiled=True),
        lax.all_gather(down_weight, "sp", axis=1, tiled=True),
    )
    tails = jnp.stack([keys[tokens - WINDOW :], values[tokens - WINDOW :]])
    before = from_behind(tails, "sp", 1)
    offset = lax.axis_index("sp") * tokens
    attended = attend(queries, keys, values, before, sinks, offset, rank_tp)
    mix = lax.psum_scatter(
        jnp.dot(attended, out_weight, preferred_element_type=jnp.float32).astype(jnp.bfloat16),
        "tp",
        scatter_dimension=0,
        tiled=True,
    ).astype(jnp.float32)
    normed = layer_norm(deep_alpha * residual.astype(jnp.float32) + mix, gains[0], biases[0])
    whole = lax.all_gather(normed, "tp", axis=0, tiled=True)
    upward = jnp.dot(whole, up_full, preferred_element_type=jnp.float32)
    act = jnp.square(jax.nn.relu(upward)).astype(jnp.bfloat16)
    terms = jnp.dot(act, down_full, preferred_element_type=jnp.float32)
    ffn = lax.psum_scatter(
        terms.astype(jnp.bfloat16), "tp", scatter_dimension=0, tiled=True
    ).astype(jnp.float32)
    return layer_norm(deep_alpha * normed.astype(jnp.float32) + ffn, gains[1], biases[1])


def solution(mesh):
    return jax.shard_map(
        on_device,
        mesh=mesh,
        in_specs=(
            P("sp", "tp"),
            P("sp", "tp"),
            P("sp", "tp"),
            P(("sp", "tp"), None),
            P("tp"),
            P("tp", None),
            P("sp", "tp"),
            P("tp", "sp"),
            P(),
            P(),
        ),
        out_specs=P(("sp", "tp"), None),
        check_vma=False,
    )
```

profile of v0, /device:TPU:0, one launch (start us, length us, event | category | flops | bytes accessed | tf_op | source)
XLA Modules:
  0.0 408.7 jit_solution(9440139312392734191)
XLA Ops:
  6.5 0.0 copy-start
  6.5 0.0 reduce-scatter.3.cloned.1.call-start
  6.5 0.9 slice_bitcast_fusion.2
  7.5 0.6 pad_maximum_fusion.2
  8.1 5.5 %collective-permute-start = (bf16[2,128,128]{2,1,0:T(8,128)(2,1)}, bf16[2,128,128]{2,1,0:T(8,128)(2,1)}, u32[]{:S(2)}, u32[]{:S(2)}) collective-permute-start(bf16[2,128,128]{2,1,0:T(8,128)(2,1)} %pad_maximum_fusion.2), channel_id=1, source_target_pairs={{0,4},{4,8},{8,12},{12,16},{16,20},{20,24},{24,28},{1,5},{5,9},{9,... | collective-permute-start | bytes 196616 | tf_op jit(solution)/shard_map/ppermute | solution.py:17
  13.8 0.1 add_compare_fusion
  13.8 0.1 broadcast_multiply_fusion
  13.9 1.0 broadcast_and_fusion
  14.9 0.0 copy-done.7
  14.9 0.2 reshape.206
  15.1 0.2 copy.14
  15.3 0.0 collective-permute-done
  15.3 0.8 slice_bitcast_fusion.1
  16.1 0.9 pad_maximum_fusion
  17.0 0.0 copy-start.10
  17.0 1.7 fusion.21
  18.7 0.1 broadcast_maximum_fusion
  18.8 1.3 copy-done.5
  20.1 0.4 fusion.1
  20.4 0.1 exponential_add_fusion
  20.5 0.2 copy.13
  20.7 2.2 fusion.2
  22.9 0.4 copy.18
  23.3 0.0 copy-done
  23.3 3.5 convolution_convert_fusion.1
  26.8 0.0 reduce-scatter.3.cloned.1.call-update
  26.9 0.0 all-gather.4.cloned.1.call-start
  26.9 0.6 copy-done.8
  27.6 39.3 %reduce-scatter.3.cloned.1.call-done = bf16[192,2048]{1,0:T(8,128)(2,1)} async-done(((bf16[768,2048]{1,0:T(8,128)(2,1)}), bf16[192,2048]{1,0:T(8,128)(2,1)}) %reduce-scatter.3.cloned.1.call-update) | async-done | bytes 786448 | tf_op jit(solution)/shard_map/reduce_scatter | solution.py:84
  66.9 1.5 fusion.3
  68.5 0.4 multiply_reduce_fusion.1
  69.0 1.4 add_convert_fusion.1
  70.3 0.0 all-gather.4.cloned.1.call-update
  70.3 0.0 all-gather.6.cloned.1.call-start
  70.4 0.7 all-gather.6.cloned.1.call-update
  71.1 0.0 all-gather.8.cloned.1.call-start
  71.1 0.5 all-gather.8.cloned.1.call-update
  71.7 0.2 reduce-scatter.5.cloned.1.call-start
  71.9 27.1 %all-gather.4.cloned.1.call-done = bf16[768,2048]{1,0:T(8,128)(2,1)} async-done(((bf16[192,2048]{1,0:T(8,128)(2,1)}), bf16[768,2048]{1,0:T(8,128)(2,1)}) %all-gather.4.cloned.1.call-update) | async-done | bytes 3145744 | tf_op jit(solution)/shard_map/all_gather | solution.py:91
  99.0 126.6 %all-gather.6.cloned.1.call-done = bf16[2048,2048]{1,0:T(8,128)(2,1)} async-done(((bf16[256,2048]{1,0:T(8,128)(2,1)}), bf16[2048,2048]{1,0:T(8,128)(2,1)}) %all-gather.6.cloned.1.call-update) | async-done | bytes 8388624 | tf_op jit(solution)/shard_map/all_gather | solution.py:77
  225.6 11.9 %multiply_convert_fusion = bf16[768,2048]{1,0:T(8,128)(2,1)} fusion(bf16[768,2048]{1,0:T(8,128)(2,1)} %all-gather.4.cloned.1.call-done, bf16[2048,2048]{1,0:T(8,128)(2,1)} %all-gather.6.cloned.1.call-done), kind=kOutput, calls=%fused_computation | convolution fusion | flops 6447169536 | bytes 14680064 | tf_op jit(solution)/shard_map/dot_general | solution.py:92
  237.5 113.2 %all-gather.8.cloned.1.call-done = bf16[2048,2048]{1,0:T(8,128)(2,1)} async-done(((bf16[2048,256]{1,0:T(8,128)(2,1)}), bf16[2048,2048]{1,0:T(8,128)(2,1)}) %all-gather.8.cloned.1.call-update) | async-done | bytes 8388624 | tf_op jit(solution)/shard_map/all_gather | solution.py:78
  350.7 11.8 %convolution_convert_fusion = bf16[768,2048]{1,0:T(8,128)(2,1)} fusion(bf16[768,2048]{1,0:T(8,128)(2,1)} %multiply_convert_fusion, bf16[2048,2048]{1,0:T(8,128)(2,1)} %all-gather.8.cloned.1.call-done), kind=kOutput, calls=%fused_computation.1 | convolution fusion | flops 6444023808 | bytes 14680064 | tf_op jit(solution)/shard_map/dot_general | solution.py:94
  362.5 0.0 reduce-scatter.5.cloned.1.call-update
  362.6 36.2 %reduce-scatter.5.cloned.1.call-done = bf16[192,2048]{1,0:T(8,128)(2,1)} async-done(((bf16[768,2048]{1,0:T(8,128)(2,1)}), bf16[192,2048]{1,0:T(8,128)(2,1)}) %reduce-scatter.5.cloned.1.call-update) | async-done | bytes 786448 | tf_op jit(solution)/shard_map/reduce_scatter | solution.py:95
  398.8 1.5 fusion.4
  400.3 0.4 multiply_reduce_fusion
  400.8 1.4 add_convert_fusion
  (28 shorter events, 0.2 us)
Async XLA Ops:
  6.5 16.8 %copy-start = (bf16[384,2048]{1,0:T(8,128)(2,1)S(1)}, bf16[384,2048]{1,0:T(8,128)(2,1)}, u32[]{:S(2)}) copy-start(bf16[384,2048]{1,0:T(8,128)(2,1)} %param.15) | copy-start | bytes 4718596
  6.5 8.5 %copy-start.6 = (bf16[768,128]{1,0:T(8,128)(2,1)S(1)}, bf16[768,128]{1,0:T(8,128)(2,1)}, u32[]{:S(2)}) copy-start(bf16[768,128]{1,0:T(8,128)(2,1)} %param.12) | copy-start | bytes 589828
  6.5 8.3 %copy-start.7 = (bf16[768,384]{1,0:T(8,128)(2,1)S(1)}, bf16[768,384]{1,0:T(8,128)(2,1)}, u32[]{:S(2)}) copy-start(bf16[768,384]{1,0:T(8,128)(2,1)} %param.10) | copy-start | bytes 1769476
  6.5 60.4 %reduce-scatter.3.cloned.1.call-start = ((), (), s32[]{:S(2)}) async-start(), calls=%async_computation.2 | async-start | bytes 3932160 | tf_op jit(solution)/shard_map/reduce_scatter | solution.py:84
  8.1 7.1 %collective-permute-start = (bf16[2,128,128]{2,1,0:T(8,128)(2,1)}, bf16[2,128,128]{2,1,0:T(8,128)(2,1)}, u32[]{:S(2)}, u32[]{:S(2)}) collective-permute-start(bf16[2,128,128]{2,1,0:T(8,128)(2,1)} %pad_maximum_fusion.2), channel_id=1, source_target_pairs={{0,4},{4,8},{8,12},{12,16},{16,20},{20,24},{24,28},{1,5},{5,9},{9,... | collective-permute-start | bytes 196616 | tf_op jit(solution)/shard_map/ppermute | solution.py:17
  17.0 1.7 copy-start.10
  18.7 1.4 copy-start.5
  26.8 0.7 copy-start.8
  26.8 0.7 copy-start.9
  26.8 40.1 %copy-start.2 = (bf16[192,2048]{1,0:T(8,128)(2,1)S(1)}, bf16[192,2048]{1,0:T(8,128)(2,1)}, u32[]{:S(2)}) copy-start(bf16[192,2048]{1,0:T(8,128)(2,1)} %param.13) | copy-start | bytes 2359300
  26.9 72.1 %all-gather.4.cloned.1.call-start = ((), (), s32[]{:S(2)}) async-start(), calls=%async_computation.3 | async-start | bytes 3932160 | tf_op jit(solution)/shard_map/all_gather | solution.py:91
  66.9 1.6 copy-start.3
  70.3 155.3 %all-gather.6.cloned.1.call-start = ((), (), s32[]{:S(2)}) async-start(), calls=%async_computation.4 | async-start | bytes 9437184 | tf_op jit(solution)/shard_map/all_gather | solution.py:77
  71.1 279.6 %all-gather.8.cloned.1.call-start = ((), (), s32[]{:S(2)}) async-start(), calls=%async_computation.5 | async-start | bytes 9437184 | tf_op jit(solution)/shard_map/all_gather | solution.py:78
  71.7 327.1 %reduce-scatter.5.cloned.1.call-start = ((), (), s32[]{:S(2)}) async-start(), calls=%async_computation.6 | async-start | bytes 3932160 | tf_op jit(solution)/shard_map/reduce_scatter | solution.py:95
  362.5 36.2 %copy-start.1 = (bf16[192,2048]{1,0:T(8,128)(2,1)S(1)}, bf16[192,2048]{1,0:T(8,128)(2,1)}, u32[]{:S(2)}) copy-start(bf16[192,2048]{1,0:T(8,128)(2,1)} %add_convert_fusion.1) | copy-start | bytes 2359300
  398.8 1.6 copy-start.4
Sparse Core Ops, SparseCore 0:
  27.0 39.9 reduce-scatter.2
  70.5 28.4 all-gather.3
  101.1 124.4 all-gather.5
  227.5 123.1 all-gather.7
  362.7 36.0 reduce-scatter.4
where the time goes:
time: 409 us
  waiting for transfers between devices  344 us (84%)
  matrix products  31.1 us (8%)
  between operations  13.3 us (3%)
  other arithmetic  10 us (2%)
  starting transfers between devices  5.86 us (1%)
  local copies, waits for them, and re-layouts  4.69 us (1%)
    all_gather x1, waiting for transfers between devices, on_device(): lax.all_gather(up_weight, 'sp', axis=0, tiled=True)  127 us
    all_gather x1, waiting for transfers between devices, on_device(): lax.all_gather(down_weight, 'sp', axis=1, tiled=True)  113 us
    reduce_scatter x1, waiting for transfers between devices, on_device(): lax.psum_scatter(jnp.dot(attended, out_weight, preferred_element_type=jnp...  39.3 us
    reduce_scatter x1, waiting for transfers between devices, on_device(): lax.psum_scatter(terms.astype(jnp.bfloat16), 'tp', scatter_dimension=0, t...  36.2 us
    all_gather x1, waiting for transfers between devices, on_device(): whole = lax.all_gather(normed, 'tp', axis=0, tiled=True)  27.1 us
    dot_general x1, matrix products, on_device(): upward = jnp.dot(whole, up_full, preferred_element_type=jnp.float32)  11.9 us
    dot_general x1, matrix products, on_device(): terms = jnp.dot(act, down_full, preferred_element_type=jnp.float32)  11.8 us
  transfers between devices with their start and end apart: 6, of which 5 were waited for; matrix products, arithmetic and copies ran while one was open for 3% of the time, Pallas kernels for 0%

commit v1 on v0

--- a/solution.py
+++ b/solution.py
@@ -88,7 +88,22 @@
         tiled=True,
     ).astype(jnp.float32)
     normed = layer_norm(deep_alpha * residual.astype(jnp.float32) + mix, gains[0], biases[0])
-    whole = lax.all_gather(normed, "tp", axis=0, tiled=True)
+
+    def try_all_joints_in(unit):
+        mesh_name = "tp"
+        axis_n = lax.axis_size(mesh_name)
+        x_new = sorted(((h, (h + 1) % axis_n) for h in range(axis_n)))
+        then = unit
+        panels = [then]
+        for k0 in tuple(range(1, axis_n)):
+            then = lax.ppermute(then, mesh_name, x_new)
+            panels.insert(0, then)
+        work_now = jnp.concatenate(panels, 0)
+        n_now = lax.axis_index(mesh_name)
+        q_next = jnp.roll(work_now, (n_now + 1) * unit.shape[0], 0)
+        return q_next
+
+    whole = try_all_joints_in(normed)
     upward = jnp.dot(whole, up_full, preferred_element_type=jnp.float32)
     act = jnp.square(jax.nn.relu(upward)).astype(jnp.bfloat16)
     terms = jnp.dot(act, down_full, preferred_element_type=jnp.float32)

time: 409 us -> 350 us (0.86)
  waiting for transfers between devices: 344 us -> 273 us
  local copies, waits for them, and re-layouts: 4.69 us -> 18.1 us
    all_gather x1, waiting for transfers between devices: 127 us -> 38.1 us  [on_device(): lax.all_gather(up_weight, 'sp', axis=0, tiled=True)]
    ppermute x0 -> x3, waiting for transfers between devices: none -> 34.6 us  [try_all_joints_in(): then = lax.ppermute(then, mesh_name, x_new)]
    all_gather x1 -> x0, waiting for transfers between devices: 27.1 us -> none  [on_device(): whole = lax.all_gather(normed, 'tp', axis=0, tiled=True)]
    dot_general x1 -> x0, matrix products: 11.9 us -> none  [on_device(): upward = jnp.dot(whole, up_full, preferred_element_type=jnp.float32)]
    all_gather x1, waiting for transfers between devices: 113 us -> 125 us  [on_device(): lax.all_gather(down_weight, 'sp', axis=1, tiled=True)]
    unnamed x22 -> x27, local copies, waits for them, and re-layouts: 2 us -> 12.6 us
    dot_general x1, matrix products: 11.8 us -> 21.5 us  [on_device(): terms = jnp.dot(act, down_full, preferred_element_type=jnp.float32)]
  transfers between devices with their start and end apart: 6 -> 8, of which waited for: 5 -> 7; matrix products, arithmetic and copies ran while one was open for 3% -> 5% of each run, Pallas kernels for 0% -> 0%
where the time goes in v1:
time: 350 us; the launch traced here: 349 us
  waiting for transfers between devices  273 us (78%)
  matrix products  27.8 us (8%)
  local copies, waits for them, and re-layouts  18.1 us (5%)
  between operations  15.1 us (4%)
  other arithmetic  9.79 us (3%)
  starting transfers between devices  5.7 us (2%)
    all_gather x1, waiting for transfers between devices, on_device(): lax.all_gather(down_weight, 'sp', axis=1, tiled=True)  125 us
    all_gather x1, waiting for transfers between devices, on_device(): lax.all_gather(up_weight, 'sp', axis=0, tiled=True)  38.1 us
    reduce_scatter x1, waiting for transfers between devices, on_device(): lax.psum_scatter(jnp.dot(attended, out_weight, preferred_element_type=jnp...  37.7 us
    reduce_scatter x1, waiting for transfers between devices, on_device(): lax.psum_scatter(terms.astype(jnp.bfloat16), 'tp', scatter_dimension=0, t...  36.2 us
    ppermute x3, waiting for transfers between devices, try_all_joints_in(): then = lax.ppermute(then, mesh_name, x_new)  34.6 us
    dot_general x1, matrix products, on_device(): terms = jnp.dot(act, down_full, preferred_element_type=jnp.float32)  21.5 us
    unnamed x27, local copies, waits for them, and re-layouts  12.6 us
  transfers between devices with their start and end apart: 8, of which 7 were waited for; matrix products, arithmetic and copies ran while one was open for 5% of the time, Pallas kernels for 0%

profile of v1, /device:TPU:0, one launch (start us, length us, event | category | flops | bytes accessed | tf_op | source)
XLA Modules:
  0.0 349.1 jit_solution(1018518502505887996)
XLA Ops:
  7.4 0.9 slice_bitcast_fusion.2
  8.3 0.6 pad_maximum_fusion.2
  9.0 5.5 %collective-permute-start = (bf16[2,128,128]{2,1,0:T(8,128)(2,1)}, bf16[2,128,128]{2,1,0:T(8,128)(2,1)}, u32[]{:S(2)}, u32[]{:S(2)}) collective-permute-start(bf16[2,128,128]{2,1,0:T(8,128)(2,1)} %pad_maximum_fusion.2), channel_id=1, source_target_pairs={{0,4},{4,8},{8,12},{12,16},{16,20},{20,24},{24,28},{1,5},{5,9},{9,... | collective-permute-start | bytes 196616 | tf_op jit(solution)/shard_map/ppermute | solution.py:17
  14.6 0.1 add_compare_fusion
  14.7 0.1 broadcast_multiply_fusion
  14.8 0.3 broadcast_and_fusion
  15.0 2.0 reshape.206
  17.1 0.2 copy.14
  17.2 0.8 slice_bitcast_fusion.1
  18.1 0.7 fusion.27
  18.7 0.1 broadcast_maximum_fusion
  18.8 1.3 copy-done.4
  20.1 0.4 fusion.2
  20.5 0.1 exponential_add_fusion
  20.6 0.2 copy.13
  20.8 2.2 fusion.3
  23.0 0.4 copy.18
  23.4 3.5 convolution_convert_fusion.1
  26.9 0.0 reduce-scatter.3.cloned.1.call-update
  26.9 0.0 all-gather.3.cloned.1.call-start
  26.9 0.5 all-gather.3.cloned.1.call-update
  27.5 0.0 all-gather.5.cloned.1.call-start
  27.5 0.5 all-gather.5.cloned.1.call-update
  28.1 0.0 reduce-scatter.5.cloned.1.call-start
  28.2 37.7 %reduce-scatter.3.cloned.1.call-done = bf16[192,2048]{1,0:T(8,128)(2,1)} async-done(((bf16[768,2048]{1,0:T(8,128)(2,1)}), bf16[192,2048]{1,0:T(8,128)(2,1)}) %reduce-scatter.3.cloned.1.call-update) | async-done | bytes 786448 | tf_op jit(solution)/shard_map/reduce_scatter | solution.py:84
  65.9 1.5 fusion.4
  67.4 1.6 multiply_reduce_fusion.1
  69.0 0.5 add_convert_fusion.1
  69.5 0.1 collective-permute-start.1
  69.6 11.4 %collective-permute-done.1 = bf16[192,2048]{1,0:T(8,128)(2,1)S(1)} collective-permute-done((bf16[192,2048]{1,0:T(8,128)(2,1)S(1)}, bf16[192,2048]{1,0:T(8,128)(2,1)S(1)}, u32[]{:S(2)}, u32[]{:S(2)}) %collective-permute-start.1) | collective-permute-done | bytes 786464 | tf_op jit(solution)/shard_map/ppermute | solution.py:99
  81.0 11.5 %collective-permute-done.2 = bf16[192,2048]{1,0:T(8,128)(2,1)} collective-permute-done((bf16[192,2048]{1,0:T(8,128)(2,1)S(1)}, bf16[192,2048]{1,0:T(8,128)(2,1)}, u32[]{:S(2)}, u32[]{:S(2)}) %collective-permute-start.2) | collective-permute-done | bytes 786464 | tf_op jit(solution)/shard_map/ppermute | solution.py:99
  92.5 11.7 %collective-permute-done.3 = bf16[192,2048]{1,0:T(8,128)(2,1)} collective-permute-done((bf16[192,2048]{1,0:T(8,128)(2,1)}, bf16[192,2048]{1,0:T(8,128)(2,1)}, u32[]{:S(2)}, u32[]{:S(2)}) %collective-permute-start.3) | collective-permute-done | bytes 786464 | tf_op jit(solution)/shard_map/ppermute | solution.py:99
  104.2 2.1 constant_dynamic-update-slice_fusion.7
  106.3 2.1 constant_dynamic-update-slice_fusion.6
  108.4 1.0 constant_dynamic-update-slice_fusion.5
  109.4 1.0 constant_dynamic-update-slice_fusion.4
  110.3 2.1 constant_dynamic-update-slice_fusion.3
  112.4 2.1 constant_dynamic-update-slice_fusion.2
  114.5 1.0 constant_dynamic-update-slice_fusion.1
  115.5 1.0 constant_dynamic-update-slice_fusion
  116.5 38.1 %all-gather.3.cloned.1.call-done = bf16[2048,2048]{1,0:T(8,128)(2,1)} async-done(((bf16[256,2048]{1,0:T(8,128)(2,1)}), bf16[2048,2048]{1,0:T(8,128)(2,1)}) %all-gather.3.cloned.1.call-update) | async-done | bytes 8388624 | tf_op jit(solution)/shard_map/all_gather | solution.py:77
  154.6 124.8 %all-gather.5.cloned.1.call-done = bf16[2048,2048]{1,0:T(8,128)(2,1)} async-done(((bf16[2048,256]{1,0:T(8,128)(2,1)}), bf16[2048,2048]{1,0:T(8,128)(2,1)}) %all-gather.5.cloned.1.call-update) | async-done | bytes 8388624 | tf_op jit(solution)/shard_map/all_gather | solution.py:78
  279.5 21.5 %convolution_convert_fusion = bf16[768,2048]{1,0:T(8,128)(2,1)} fusion(bf16[2048,2048]{1,0:T(8,128)(2,1)} %all-gather.5.cloned.1.call-done, bf16[2048,2048]{1,0:T(8,128)(2,1)} %all-gather.3.cloned.1.call-done, bf16[1536,2048]{1,0:T(8,128)(2,1)} %constant_dynamic-update-slice_fusion, s32[]{:T(128)S(6)} %select_n.19), kind=kOutput, calls=%fused_computation.1 | convolution fusion | flops 12891193344 | bytes 23068676 | tf_op jit(solution)/shard_map/dot_general | solution.py:109
  301.0 0.0 reduce-scatter.5.cloned.1.call-update
  301.0 36.2 %reduce-scatter.5.cloned.1.call-done = bf16[192,2048]{1,0:T(8,128)(2,1)} async-done(((bf16[768,2048]{1,0:T(8,128)(2,1)}), bf16[192,2048]{1,0:T(8,128)(2,1)}) %reduce-scatter.5.cloned.1.call-update) | async-done | bytes 786448 | tf_op jit(solution)/shard_map/reduce_scatter | solution.py:110
  337.2 1.5 fusion.5
  338.8 1.6 multiply_reduce_fusion
  340.3 1.3 add_convert_fusion
  (36 shorter events, 0.2 us)
Async XLA Ops:
  7.4 16.0 %copy-start = (bf16[384,2048]{1,0:T(8,128)(2,1)S(1)}, bf16[384,2048]{1,0:T(8,128)(2,1)}, u32[]{:S(2)}) copy-start(bf16[384,2048]{1,0:T(8,128)(2,1)} %param.15) | copy-start | bytes 4718596
  7.4 10.7 %copy-start.6 = (bf16[768,128]{1,0:T(8,128)(2,1)S(1)}, bf16[768,128]{1,0:T(8,128)(2,1)}, u32[]{:S(2)}) copy-start(bf16[768,128]{1,0:T(8,128)(2,1)} %param.11) | copy-start | bytes 589828
  7.4 9.7 %copy-start.5 = (bf16[768,128]{1,0:T(8,128)(2,1)S(1)}, bf16[768,128]{1,0:T(8,128)(2,1)}, u32[]{:S(2)}) copy-start(bf16[768,128]{1,0:T(8,128)(2,1)} %param.12) | copy-start | bytes 589828
  7.4 58.5 %reduce-scatter.3.cloned.1.call-start = ((), (), s32[]{:S(2)}) async-start(), calls=%async_computation.2 | async-start | bytes 3932160 | tf_op jit(solution)/shard_map/reduce_scatter | solution.py:84
  9.0 8.3 %collective-permute-start = (bf16[2,128,128]{2,1,0:T(8,128)(2,1)}, bf16[2,128,128]{2,1,0:T(8,128)(2,1)}, u32[]{:S(2)}, u32[]{:S(2)}) collective-permute-start(bf16[2,128,128]{2,1,0:T(8,128)(2,1)} %pad_maximum_fusion.2), channel_id=1, source_target_pairs={{0,4},{4,8},{8,12},{12,16},{16,20},{20,24},{24,28},{1,5},{5,9},{9,... | collective-permute-start | bytes 196616 | tf_op jit(solution)/shard_map/ppermute | solution.py:17
  18.0 0.7 copy-start.9
  18.7 1.4 copy-start.4
  26.9 1.3 copy-start.7
  26.9 1.3 copy-start.8
  26.9 39.0 %copy-start.1 = (bf16[192,2048]{1,0:T(8,128)(2,1)S(1)}, bf16[192,2048]{1,0:T(8,128)(2,1)}, u32[]{:S(2)}) copy-start(bf16[192,2048]{1,0:T(8,128)(2,1)} %param.13) | copy-start | bytes 2359300
  26.9 127.7 %all-gather.3.cloned.1.call-start = ((), (), s32[]{:S(2)}) async-start(), calls=%async_computation.3 | async-start | bytes 9437184 | tf_op jit(solution)/shard_map/all_gather | solution.py:77
  27.5 252.0 %all-gather.5.cloned.1.call-start = ((), (), s32[]{:S(2)}) async-start(), calls=%async_computation.4 | async-start | bytes 9437184 | tf_op jit(solution)/shard_map/all_gather | solution.py:78
  28.1 309.1 %reduce-scatter.5.cloned.1.call-start = ((), (), s32[]{:S(2)}) async-start(), calls=%async_computation.5 | async-start | bytes 3932160 | tf_op jit(solution)/shard_map/reduce_scatter | solution.py:110
  65.9 3.1 copy-start.2
  69.5 11.5 %collective-permute-start.1 = (bf16[192,2048]{1,0:T(8,128)(2,1)S(1)}, bf16[192,2048]{1,0:T(8,128)(2,1)S(1)}, u32[]{:S(2)}, u32[]{:S(2)}) collective-permute-start(bf16[192,2048]{1,0:T(8,128)(2,1)S(1)} %add_convert_fusion.1), channel_id=1, source_target_pairs={{0,1},{1,2},{2,3},{3,0},{4,5},{5,6},{6,7},{7,4},{8,9},{9,10},{10,1... | collective-permute-start | bytes 2359304 | tf_op jit(solution)/shard_map/ppermute | solution.py:99
  81.0 11.5 %collective-permute-start.2 = (bf16[192,2048]{1,0:T(8,128)(2,1)S(1)}, bf16[192,2048]{1,0:T(8,128)(2,1)}, u32[]{:S(2)}, u32[]{:S(2)}) collective-permute-start(bf16[192,2048]{1,0:T(8,128)(2,1)S(1)} %collective-permute-done.1), channel_id=1, source_target_pairs={{0,1},{1,2},{2,3},{3,0},{4,5},{5,6},{6,7},{7,4},{8,9},{9,10},{10,1... | collective-permute-start | bytes 2359304 | tf_op jit(solution)/shard_map/ppermute | solution.py:99
  92.5 11.7 %collective-permute-start.3 = (bf16[192,2048]{1,0:T(8,128)(2,1)}, bf16[192,2048]{1,0:T(8,128)(2,1)}, u32[]{:S(2)}, u32[]{:S(2)}) collective-permute-start(bf16[192,2048]{1,0:T(8,128)(2,1)} %collective-permute-done.2), channel_id=1, source_target_pairs={{0,1},{1,2},{2,3},{3,0},{4,5},{5,6},{6,7},{7,4},{8,9},{9,10},{10,1... | collective-permute-start | bytes 2359304 | tf_op jit(solution)/shard_map/ppermute | solution.py:99
  337.2 3.1 copy-start.3
Sparse Core Ops, SparseCore 0:
  27.0 38.7 reduce-scatter.2
  301.1 36.0 reduce-scatter.4
Sparse Core Ops, SparseCore 1:
  29.5 125.0 all-gather.2
  156.5 122.9 all-gather.4
